TPU v7x, 256 devices: a whole 4x4x8 slice. The times are simulated.
256 devices in a mesh: sp: 32 (over z, y), tp: 8 (over x, core).
Axes of the slice: x: 4, y: 4, z: 8, core: 2. Of those that a mesh axis runs over, the one named last changes fastest.
Arguments:
- tokens: bfloat16 [32768, 4096], P('sp', 'tp'), may hold values from -6 to 6
- norm_gain: float32 [4096], replicated, may hold values from 0.1 to 1.9
- pool_in_weight: bfloat16 [4096, 2048], P('sp', 'tp'), may hold values from -0.09375 to 0.09375
- query_weight: bfloat16 [4096, 2048], P('sp', 'tp'), may hold values from -1 to 1, as said below
- key_weight: bfloat16 [4096, 512], P('sp', 'tp'), may hold values from -40 to 40
- value_weight: bfloat16 [4096, 512], P('sp', 'tp'), may hold values from -0.09375 to 0.09375
- pool_weight: bfloat16 [8, 256, 256], P('tp'), may hold values from -0.375 to 0.375
- pool_scale: float32 [2048], P('tp'), may hold values from 0.1 to 1.9
- sink_logit: float32 [32], P('tp'), may hold values from 3 to 7
- out_pool_weight: bfloat16 [2048, 4096], P('tp', 'sp'), may hold values from -0.09375 to 0.09375
- out_attn_weight: bfloat16 [2048, 4096], P('tp', 'sp'), may hold values from -1.5 to 1.5
Outputs:
- mixed: bfloat16 [32768, 4096], P(('sp', 'tp'))
Inputs may be any that keep to these rules, and one draw needn't show every extreme that they name: `query_weight`: entries of order 4096 ** -0.5, drawn independently.
All inputs are finite; a program needn't handle non-finite values.
Results may differ from a plain program's by a relative error of at most 0.014.
The roundings to bfloat16 on the way count: a program that leaves them out, or rounds other values in their place, can miss the bound.
Values may be sent and summed in bfloat16 or wider, within the bound.
No kernel may reach another device: no remote copies, remote signals or barrier semaphores. Data moves between devices by JAX's collectives and lax.ppermute only.
A program may use at most 128 MiB of HBM per device.

v0:
```python
import jax
import jax.numpy as jnp
from jax import lax
from jax.sharding import Mesh
from jax.sharding import PartitionSpec as P

HEAD_DIM = 64
Q_HEADS = 32
KV_HEADS = 8
GROUP_DIM = 256
WINDOW = 128
GRID_W = 64
SP = ("sp_0", "sp_1")
SP_TP = ("sp_0", "sp_1", "tp")
epsilon = 1e-06
rotary_base = 10000.0
masked_score = -1e30


def sent_together(arrays, axis, dim, along):
    widths = [a.shape[along] for a in arrays]
    both = jnp.concatenate(arrays, axis=along)
    result = lax.all_gather(both, axis, axis=dim, tiled=True)
    return tuple(jnp.split(result, [sum(widths[:k]) for k in range(1, len(widths))], axis=along))


def padded_2(block, sides, width):
    for axis, dim in sides:
        count = lax.axis_size(axis)
        forward = [(i, i + 1) for i in range(count - 1)]
        backward = [(target, source) for source, target in forward]
        low = lax.ppermute(
            lax.slice_in_dim(block, block.shape[dim] - width, None, axis=dim), axis, forward
        )
        high = lax.ppermute(lax.slice_in_dim(block, 0, width, axis=dim), axis, backward)
        block = jnp.concatenate([low, block, high], axis=dim)
    return block


def gather_axes(array, axes, dim):
    if not axes:
        return array
    nearer = lax.all_gather(array, axes[-1], axis=dim, tiled=True)
    return gather_axes(nearer, axes[:-1], dim)


def rms_normed(values, gain):
    floats = values.astype(jnp.float32)
    scaled = floats * lax.rsqrt(jnp.mean(floats * floats, axis=-1, keepdims=True) + epsilon)
    return (scaled * gain).astype(jnp.bfloat16)


def rotary_tables(positions, head_dim, grid_width):
    freq_count = head_dim // 4
    inverse = rotary_base ** (-jnp.arange(freq_count, dtype=jnp.float32) / freq_count)
    row_pos = (positions // grid_width).astype(jnp.float32)
    col_pos = (positions % grid_width).astype(jnp.float32)
    angles = jnp.stack([row_pos[:, None] * inverse, col_pos[:, None] * inverse], axis=1)
    return (jnp.cos(angles), jnp.sin(angles))


def rotate(values, cosine, sine):
    length, heads, head_dim = values.shape
    split = values.reshape(length, heads, 2, 2, head_dim // 4)
    first = split[:, :, :, 0]
    second = split[:, :, :, 1]
    cos_b = cosine[:, None]
    sin_b = sine[:, None]
    turned = jnp.stack([first * cos_b - second * sin_b, second * cos_b + first * sin_b], axis=3)
    return turned.reshape(length, heads, head_dim)


def shards(
    tokens,
    norm_gain,
    pool_in_weight,
    query_weight,
    key_weight,
    value_weight,
    pool_weight,
    pool_scale,
    sink_logit,
    out_pool_weight,
    out_attn_weight,
):
    whole_rows = lax.all_gather(tokens, "tp", axis=1, tiled=True)
    normed = rms_normed(whole_rows, norm_gain)
    tok_rows = normed.shape[0]

    def project(piece):
        return jnp.dot(normed, piece, preferred_element_type=jnp.float32)

    pieces = sent_together((pool_in_weight, query_weight, key_weight, value_weight), SP, 0, 1)
    pool_raw, query_raw, key_raw, value_raw = tuple((project(piece) for piece in pieces))
    sp_index = lax.axis_index(SP)
    tp_index = lax.axis_index("tp")
    total_rows = tok_rows * lax.axis_size(SP)
    offset = sp_index * tok_rows
    positions = offset + jnp.arange(tok_rows, dtype=jnp.int32)
    cosine, sine = rotary_tables(positions, HEAD_DIM, GRID_W)
    pool_in = pool_raw.astype(jnp.bfloat16)
    queries = rotate(query_raw.reshape(tok_rows, -1, HEAD_DIM), cosine, sine).astype(jnp.bfloat16)
    key_part = rotate(key_raw.reshape(tok_rows, -1, HEAD_DIM), cosine, sine).astype(jnp.bfloat16)
    key_part = key_part.reshape(tok_rows, -1)
    value_part = value_raw.astype(jnp.bfloat16)
    kv_rows = jnp.concatenate([key_part, value_part], axis=1)
    kv_width = key_part.shape[1]
    channels = pool_in.shape[1]
    pool_reach = 8
    rim_depth = max(WINDOW, pool_reach)
    padded = padded_2(jnp.concatenate([pool_in, kv_rows], axis=1), ((SP, 0),), rim_depth)
    pool_pad = padded[rim_depth - pool_reach : rim_depth + tok_rows + pool_reach, :channels]
    kv_pad = padded[rim_depth - WINDOW : rim_depth + tok_rows + WINDOW, channels:]
    running = jnp.concatenate(
        [jnp.zeros((1, channels), jnp.float32), jnp.cumsum(pool_pad.astype(jnp.float32), axis=0)],
        axis=0,
    )
    groups_dev = channels // GROUP_DIM
    selector = (tp_index * groups_dev + jnp.arange(channels, dtype=jnp.int32) // GROUP_DIM) % 4
    window_mean = jnp.zeros((tok_rows, channels), jnp.float32)
    for level, half_width in enumerate((1, 2, 4, 8)):
        window_sum = (
            running[pool_reach + half_width : pool_reach + half_width + tok_rows]
            - running[pool_reach - half_width : pool_reach - half_width + tok_rows]
        )
        counts = jnp.minimum(positions + half_width, total_rows) - jnp.maximum(
            positions - half_width, 0
        )
        level_mean = window_sum / counts.astype(jnp.float32)[:, None]
        window_mean = jnp.where((selector == level)[None, :], level_mean, window_mean)
    pooled = (window_mean - pool_in.astype(jnp.float32)).astype(jnp.bfloat16)
    mixing = jnp.einsum(
        "tgc,gcd->tgd",
        pooled.reshape(tok_rows, groups_dev, GROUP_DIM),
        pool_weight,
        preferred_element_type=jnp.float32,
    )
    pool_out = (mixing.reshape(tok_rows, channels) * pool_scale).astype(jnp.bfloat16)
    group = Q_HEADS // KV_HEADS
    kv_heads_dev = kv_width // HEAD_DIM
    query_groups = queries.reshape(tok_rows, kv_heads_dev, group, HEAD_DIM)
    key_pad = kv_pad[:, :kv_width].reshape(-1, kv_heads_dev, HEAD_DIM)
    value_pad = kv_pad[:, kv_width:].reshape(-1, kv_heads_dev, HEAD_DIM)
    scores = jnp.einsum(
        "qkgd,skd->kgqs", query_groups, key_pad, preferred_element_type=jnp.float32
    ) * HEAD_DIM ** (-0.5)
    key_pos = offset - WINDOW + jnp.arange(tok_rows + 2 * WINDOW, dtype=jnp.int32)
    allowed = (
        (jnp.abs(key_pos[None, :] - positions[:, None]) <= WINDOW)
        & (key_pos >= 0)[None, :]
        & (key_pos < total_rows)[None, :]
    )
    scores = jnp.where(allowed, scores, masked_score)
    sink = sink_logit.reshape(kv_heads_dev, group, 1, 1)
    highest = jnp.maximum(jnp.max(scores, axis=-1, keepdims=True), sink)
    expo = jnp.exp(scores - highest)
    denominator = jnp.sum(expo, axis=-1, keepdims=True) + jnp.exp(sink - highest)
    weights = (expo / denominator).astype(jnp.bfloat16)
    attended = jnp.einsum("kgqs,skd->qkgd", weights, value_pad, preferred_element_type=jnp.float32)
    attn_out = attended.reshape(tok_rows, -1).astype(jnp.bfloat16)
    out_pool_full, out_attn_full = (
        gather_axes(out_pool_weight, SP, 1),
        gather_axes(out_attn_weight, SP, 1),
    )
    return lax.psum_scatter(
        (
            jnp.dot(pool_out, out_pool_full, preferred_element_type=jnp.float32)
            + jnp.dot(attn_out, out_attn_full, preferred_element_type=jnp.float32)
        ).astype(jnp.bfloat16),
        "tp",
        scatter_dimension=0,
        tiled=True,
    )


def solution(mesh):
    finer = Mesh(mesh.devices.reshape(8, 4, mesh.shape["tp"]), ("sp_0", "sp_1", "tp"))
    return jax.shard_map(
        shards,
        mesh=finer,
        in_specs=(
            P(SP, "tp"),
            P(),
            P(SP, "tp"),
            P(SP, "tp"),
            P(SP, "tp"),
            P(SP, "tp"),
            P("tp", None, None),
            P("tp"),
            P("tp"),
            P("tp", SP),
            P("tp", SP),
        ),
        out_specs=P(SP_TP, None),
        check_vma=False,
    )
```

profile of v0, /device:TPU:1, one launch (start us, length us, event | category | flops | bytes accessed | tf_op | source)
XLA Modules:
  0.0 306.1 jit_solution(10103627928105953874)
XLA Ops:
  6.5 0.0 copy-start
  6.5 0.0 all-gather.5.cloned.1.call-start
  6.5 0.7 all-gather.5.cloned.1.call-update
  7.3 0.0 all-gather.7.cloned.1.call-start
  7.3 0.8 copy.17
  8.1 0.8 copy.18
  9.0 1.6 pad_maximum_fusion.2
  10.6 0.0 all-gather.7.cloned.1.call-update
  10.6 0.0 all-gather.9.cloned.1.call-start
  10.7 12.0 %all_gather.20 = bf16[256,512]{1,0:T(8,128)(2,1)} all-gather(bf16[256,128]{1,0:T(8,128)(2,1)} %param.20), channel_id=1, replica_groups=mesh['sp_0'=8,'sp_1'=4,'tp'=8] {'sp_1'}, dimensions={1}, use_global_device_ids=true | all-gather | bytes 327680 | tf_op jit(solution)/shard_map/all_gather | solution.py:43
  22.7 0.0 all-gather.9.cloned.1.call-update
  22.7 0.0 all-gather.11.cloned.1.call-start
  22.7 11.1 %all_gather.22 = bf16[256,512]{1,0:T(8,128)(2,1)} all-gather(bf16[256,128]{1,0:T(8,128)(2,1)} %param.21), channel_id=1, replica_groups=mesh['sp_0'=8,'sp_1'=4,'tp'=8] {'sp_1'}, dimensions={1}, use_global_device_ids=true | all-gather | bytes 327680 | tf_op jit(solution)/shard_map/all_gather | solution.py:43
  33.8 0.0 all-gather.11.cloned.1.call-update
  33.8 0.0 copy-start.13
  33.8 0.0 reduce-scatter.2.cloned.1.call-start
  34.0 0.6 broadcast_compare_fusion
  34.6 0.6 broadcast_compare_fusion.2
  35.2 0.1 broadcast_multiply_fusion.1
  35.3 0.5 fusion.76
  35.7 3.1 fusion.7
  38.8 26.8 %all-gather.5.cloned.1.call-done = bf16[1024,4096]{1,0:T(8,128)(2,1)} async-done(((bf16[1024,512]{1,0:T(8,128)(2,1)}), bf16[1024,4096]{1,0:T(8,128)(2,1)}) %all-gather.5.cloned.1.call-update) | async-done | bytes 8388624 | tf_op jit(solution)/shard_map/all_gather | solution.py:86
  65.6 5.1 %fusion.1 = f32[1024]{0:T(1024)S(1)} fusion(bf16[1024,4096]{1,0:T(8,128)(2,1)} %all-gather.5.cloned.1.call-done), kind=kLoop, calls=%fused_computation.6 | loop fusion | flops 12581888 | bytes 8392704 | tf_op jit(solution)/shard_map/reduce_sum | solution.py:49
  70.7 10.3 %fusion.3 = bf16[1024,4096]{1,0:T(8,128)(2,1)} fusion(bf16[1024,4096]{1,0:T(8,128)(2,1)} %all-gather.5.cloned.1.call-done, f32[4096]{0:T(1024)S(1)} %copy-done.13, f32[1024]{0:T(1024)S(1)} %add_rsqrt_fusion), kind=kLoop, calls=%fused_computation.8 | loop fusion | flops 16777216 | bytes 16797696 | tf_op jit(solution)/shard_map/convert_element_type | solution.py:50
  81.0 68.8 %all-gather.7.cloned.1.call-done = bf16[4096,640]{1,0:T(8,128)(2,1)} async-done(((bf16[128,640]{1,0:T(8,128)(2,1)}), bf16[4096,640]{1,0:T(8,128)(2,1)}) %all-gather.7.cloned.1.call-update) | async-done | bytes 5242896 | tf_op jit(solution)/shard_map/all_gather | solution.py:23
  149.9 6.4 %fusion.33 = f32[1024,64]{0,1:T(8,128)S(1)} fusion(bf16[1024,4096]{1,0:T(8,128)(2,1)} %fusion.3, bf16[4096,640]{1,0:T(8,128)(2,1)} %all-gather.7.cloned.1.call-done), kind=kOutput, calls=%fused_computation.42 | convolution fusion | flops 536870912 | bytes 9699328 | tf_op jit(solution)/shard_map/dot_general | solution.py:91
  156.3 0.5 subtract_convert_fusion.1
  156.8 0.6 copy-done.8
  157.4 2.4 fusion.14
  159.8 0.0 copy-start.4
  159.8 2.7 convolution_convert_fusion
  162.6 1.9 collective-permute-start
  164.5 1.5 collective-permute-start.1
  166.0 2.4 fusion.8
  168.4 0.2 subtract_convert_fusion
  168.5 0.8 pad_maximum_fusion.1
  169.4 0.0 collective-permute-done
  169.4 0.9 collective-permute-done.1
  170.3 0.1 pad_maximum_fusion
  170.4 0.5 copy-done.11
  170.9 0.2 slice_bitcast_fusion
  171.2 0.1 pad_convert_fusion
  171.2 0.4 copy.19
  171.6 1.3 fusion.12
  172.9 0.2 broadcast_add_fusion
  173.2 0.0 copy-start.14
  173.2 5.2 %fusion.96 = (f32[4,1024]{1,0:T(4,128)S(1)}, f32[1,4,1024,1280]{2,3,1,0:T(8,128)S(1)}) fusion(bf16[1024,4,64]{0,2,1:T(8,128)(2,1)} %bitcast.62, bf16[128,384]{0,1:T(8,128)(2,1)} %copy-done.11, bf16[128,384]{0,1:T(8,128)(2,1)} %copy-done.9, bf16[1024,64]{0,1:T(8,128)(2,1)S(1)} %convolution_convert_fusion, bf16[1024,64]{0,1:T(8,128)(2,1)} %bitcast.59, ...), kind=kOutput, calls=%fused_computation.140 | convolution fusion | flops 687632384 | bytes 23805952 | tf_op jit(solution)/shard_map/qkgd,skd->kgqs/dot_general | solution.py:144
  178.4 0.0 copy-start.3
  178.4 0.0 copy-done.14
  178.4 0.1 broadcast_maximum_fusion
  178.5 3.0 fusion
  181.5 4.0 %copy-done.3 = f32[1,4,1024,1280]{2,3,1,0:T(8,128)} copy-done((f32[1,4,1024,1280]{2,3,1,0:T(8,128)}, f32[1,4,1024,1280]{2,3,1,0:T(8,128)S(1)}, u32[]{:S(2)}) %copy-start.3) | copy-done | bytes 20971544
  185.5 0.1 exponential_add_fusion
  185.6 0.7 copy.21
  186.3 0.4 copy.22
  186.7 3.0 all-gather.9.cloned.1.call-done
  189.7 0.0 copy-done.5
  189.7 0.0 copy-done.16
  189.8 10.7 %fusion.21 = f32[1024,4096]{1,0:T(8,128)} fusion(bf16[256,4096]{1,0:T(8,128)(2,1)} %all-gather.9.cloned.1.call-done, bf16[1024,256]{0,1:T(8,128)(2,1)S(1)} %copy-done.5, f32[1152,256]{0,1:T(8,128)S(1)} %bitcast.55, f32[1040,256]{0,1:T(8,128)S(1)} %bitcast.56, f32[256]{0:T(256)S(1)} %copy-done.15, f32[1024]{0:T(1024)S(1)} %get-tuple-element.23, ...), kind=kOutput, calls=%fused_computation.25 | convolution fusion | flops 2286157824 | bytes 28068864 | tf_op jit(solution)/shard_map/dot_general | solution.py:167
  200.5 9.3 %fusion.18 = bf16[64,4,1024]{2,0,1:T(8,128)(2,1)S(1)} fusion(f32[4,1024]{1,0:T(4,128)S(1)} %exponential_add_fusion, f32[1,4,1024,1280]{2,3,1,0:T(8,128)} %copy-done.3, f32[4,1024]{1,0:T(4,128)S(1)} %broadcast_maximum_fusion, bf16[128,384]{0,1:T(8,128)(2,1)S(1)} %copy-done.12, bf16[128,384]{0,1:T(8,128)(2,1)S(1)} %copy-done.10, ...), kind=kOutput, calls=%fused_computation.24 | convolution fusion | flops 687898624 | bytes 22511616 | tf_op jit(solution)/shard_map/kgqs,skd->qkgd/dot_general | solution.py:159
  209.8 20.3 %all-gather.11.cloned.1.call-done = bf16[256,4096]{1,0:T(8,128)(2,1)} async-done(((bf16[256,512]{1,0:T(8,128)(2,1)}), bf16[256,4096]{1,0:T(8,128)(2,1)}) %all-gather.11.cloned.1.call-update) | async-done | bytes 2097168 | tf_op jit(solution)/shard_map/all_gather | solution.py:43
  230.1 12.1 %add_convert_fusion = bf16[1024,4096]{1,0:T(8,128)(2,1)} fusion(f32[1024,4096]{1,0:T(8,128)} %fusion.21, bf16[1024,256]{0,1:T(8,128)(2,1)S(1)} %bitcast.54, bf16[256,4096]{1,0:T(8,128)(2,1)} %all-gather.11.cloned.1.call-done), kind=kOutput, calls=%fused_computation.9 | convolution fusion | flops 2155872256 | bytes 27787264 | tf_op jit(solution)/shard_map/dot_general | solution.py:168
  242.2 0.0 reduce-scatter.2.cloned.1.call-update
  242.2 57.4 %reduce-scatter.2.cloned.1.call-done = bf16[128,4096]{1,0:T(8,128)(2,1)} async-done(((bf16[1024,4096]{1,0:T(8,128)(2,1)}), bf16[128,4096]{1,0:T(8,128)(2,1)}) %reduce-scatter.2.cloned.1.call-update) | async-done | bytes 1048592 | tf_op jit(solution)/shard_map/reduce_scatter | solution.py:165
  (41 shorter events, 0.2 us)
Async XLA Ops:
  6.5 183.2 %copy-start = (bf16[1,256,256]{2,1,0:T(8,128)(2,1)S(1)}, bf16[1,256,256]{2,1,0:T(8,128)(2,1)}, u32[]{:S(2)}) copy-start(bf16[1,256,256]{2,1,0:T(8,128)(2,1)} %param.17) | copy-start | bytes 393220
  6.5 59.1 %all-gather.5.cloned.1.call-start = ((), (), s32[]{:S(2)}) async-start(), calls=%async_computation.1 | async-start | bytes 9437184 | tf_op jit(solution)/shard_map/all_gather | solution.py:86
  7.3 142.6 %all-gather.7.cloned.1.call-start = ((), (), s32[]{:S(2)}) async-start(), calls=%async_computation.2 | async-start | bytes 5406720 | tf_op jit(solution)/shard_map/all_gather | solution.py:23
  10.6 179.1 %all-gather.9.cloned.1.call-start = ((), (), s32[]{:S(2)}) async-start(), calls=%async_computation.3 | async-start | bytes 2359296 | tf_op jit(solution)/shard_map/all_gather | solution.py:43
  22.7 207.4 %all-gather.11.cloned.1.call-start = ((), (), s32[]{:S(2)}) async-start(), calls=%async_computation.4 | async-start | bytes 2359296 | tf_op jit(solution)/shard_map/all_gather | solution.py:43
  33.8 36.9 %copy-start.13 = (f32[4096]{0:T(1024)S(1)}, f32[4096]{0:T(1024)}, u32[]{:S(2)}) copy-start(f32[4096]{0:T(1024)} %param.12) | copy-start | bytes 49156
  33.8 265.8 %reduce-scatter.2.cloned.1.call-start = ((), (), s32[]{:S(2)}) async-start(), calls=%async_computation.5 | async-start | bytes 9437184 | tf_op jit(solution)/shard_map/reduce_scatter | solution.py:165
  149.8 6.9 %copy-start.2 = (bf16[1024,4096]{1,0:T(8,128)(2,1)S(1)}, bf16[1024,4096]{1,0:T(8,128)(2,1)}, u32[]{:S(2)}) copy-start(bf16[1024,4096]{1,0:T(8,128)(2,1)} %fusion.3) | copy-start | bytes 25165828
  149.9 7.6 %copy-start.8 = (bf16[4096,640]{1,0:T(8,128)(2,1)S(1)}, bf16[4096,640]{1,0:T(8,128)(2,1)}, u32[]{:S(2)}) copy-start(bf16[4096,640]{1,0:T(8,128)(2,1)} %all-gather.7.cloned.1.call-done) | copy-start | bytes 15728644
  157.4 12.8 %copy-start.6 = (bf16[1024,1,2,2,16]{0,4,3,2,1:T(8,128)(2,1)}, bf16[1024,1,2,2,16]{0,4,3,2,1:T(8,128)(2,1)S(1)}, u32[]{:S(2)}) copy-start(bf16[1024,1,2,2,16]{0,4,3,2,1:T(8,128)(2,1)S(1)} %pad_maximum_fusion.4) | copy-start | bytes 393220
  159.8 10.4 %copy-start.4 = (bf16[1024,256]{0,1:T(8,128)(2,1)}, bf16[1024,256]{0,1:T(8,128)(2,1)S(1)}, u32[]{:S(2)}) copy-start(bf16[1024,256]{0,1:T(8,128)(2,1)S(1)} %fusion.14) | copy-start | bytes 1572868
  162.6 6.8 %collective-permute-start = (bf16[128,384]{0,1:T(8,128)(2,1)S(1)}, bf16[128,384]{0,1:T(8,128)(2,1)S(1)}, u32[]{:S(2)}, u32[]{:S(2)}) collective-permute-start(bf16[128,384]{0,1:T(8,128)(2,1)S(1)} %get-tuple-element.7), channel_id=1, source_target_pairs={{0,8},{8,16},{16,24},{24,32},{32,40},{40,48},{48,56},{56,64},{64,7... | collective-permute-start | bytes 294920 | tf_op jit(solution)/shard_map/ppermute | solution.py:32
  164.5 5.8 %collective-permute-start.1 = (bf16[128,384]{0,1:T(8,128)(2,1)S(1)}, bf16[128,384]{0,1:T(8,128)(2,1)S(1)}, u32[]{:S(2)}, u32[]{:S(2)}) collective-permute-start(bf16[128,384]{0,1:T(8,128)(2,1)S(1)} %get-tuple-element.8), channel_id=1, source_target_pairs={{8,0},{16,8},{24,16},{32,24},{40,32},{48,40},{56,48},{64,56},{72,6... | collective-permute-start | bytes 294920 | tf_op jit(solution)/shard_map/ppermute | solution.py:35
  169.4 1.0 copy-start.9
  170.3 0.6 copy-start.11
  173.2 5.2 %copy-start.14 = (f32[4]{0:T(128)S(1)}, f32[4]{0:T(128)}, u32[]{:S(2)}) copy-start(f32[4]{0:T(128)} %param.19) | copy-start | bytes 52
  178.4 7.1 %copy-start.3 = (f32[1,4,1024,1280]{2,3,1,0:T(8,128)}, f32[1,4,1024,1280]{2,3,1,0:T(8,128)S(1)}, u32[]{:S(2)}) copy-start(f32[1,4,1024,1280]{2,3,1,0:T(8,128)S(1)} %get-tuple-element.20) | copy-start | bytes 62914564
  185.5 4.2 %copy-start.5 = (bf16[1024,256]{0,1:T(8,128)(2,1)S(1)}, bf16[1024,256]{0,1:T(8,128)(2,1)}, u32[]{:S(2)}) copy-start(bf16[1024,256]{0,1:T(8,128)(2,1)} %copy-done.4) | copy-start | bytes 1572868
  185.5 4.2 %copy-start.15 = (f32[256]{0:T(256)S(1)}, f32[256]{0:T(256)}, u32[]{:S(2)}) copy-start(f32[256]{0:T(256)} %param.18) | copy-start | bytes 3076
  185.5 4.2 %copy-start.16 = (pred[256]{0:T(512)(128)(4,1)S(1)}, pred[256]{0:T(512)(128)(4,1)}, u32[]{:S(2)}) copy-start(pred[256]{0:T(512)(128)(4,1)} %get-tuple-element.27) | copy-start | bytes 772
  185.5 4.2 %copy-start.17 = (pred[256]{0:T(512)(128)(4,1)S(1)}, pred[256]{0:T(512)(128)(4,1)}, u32[]{:S(2)}) copy-start(pred[256]{0:T(512)(128)(4,1)} %get-tuple-element.28) | copy-start | bytes 772
  185.6 4.2 %copy-start.18 = (pred[256]{0:T(512)(128)(4,1)S(1)}, pred[256]{0:T(512)(128)(4,1)}, u32[]{:S(2)}) copy-start(pred[256]{0:T(512)(128)(4,1)} %get-tuple-element.29) | copy-start | bytes 772
  185.6 4.2 %copy-start.19 = (pred[256]{0:T(512)(128)(4,1)S(1)}, pred[256]{0:T(512)(128)(4,1)}, u32[]{:S(2)}) copy-start(pred[256]{0:T(512)(128)(4,1)} %get-tuple-element.30) | copy-start | bytes 772
  189.8 10.7 %copy-start.7 = (bf16[1024,1,2,2,16]{0,4,3,2,1:T(8,128)(2,1)S(1)}, bf16[1024,1,2,2,16]{0,4,3,2,1:T(8,128)(2,1)}, u32[]{:S(2)}) copy-start(bf16[1024,1,2,2,16]{0,4,3,2,1:T(8,128)(2,1)} %copy-done.6) | copy-start | bytes 393220
  189.8 10.7 %copy-start.10 = (bf16[128,384]{0,1:T(8,128)(2,1)S(1)}, bf16[128,384]{0,1:T(8,128)(2,1)}, u32[]{:S(2)}) copy-start(bf16[128,384]{0,1:T(8,128)(2,1)} %copy-done.9) | copy-start | bytes 294916
  189.8 10.7 %copy-start.12 = (bf16[128,384]{0,1:T(8,128)(2,1)S(1)}, bf16[128,384]{0,1:T(8,128)(2,1)}, u32[]{:S(2)}) copy-start(bf16[128,384]{0,1:T(8,128)(2,1)} %copy-done.11) | copy-start | bytes 294916
  230.1 69.5 %copy-start.1 = (bf16[1,256,256]{2,1,0:T(8,128)(2,1)S(1)}, bf16[1,256,256]{2,1,0:T(8,128)(2,1)}, u32[]{:S(2)}) copy-start(bf16[1,256,256]{2,1,0:T(8,128)(2,1)} %param.17) | copy-start | bytes 393220
Sparse Core Ops, SparseCore 0:
  9.2 56.4 all-gather.4
  68.2 81.6 all-gather.6
  151.6 38.0 all-gather.8
  191.4 38.6 all-gather.10
  242.3 57.2 reduce-scatter.1
where the time goes:
time: 307 us; the launch traced here: 306 us
  waiting for transfers between devices  178 us (58%)
  matrix products  51.3 us (17%)
  other arithmetic  28.3 us (9%)
  blocking collectives  23 us (7%)
  between operations  13.5 us (4%)
  local copies, waits for them, and re-layouts  8.52 us (3%)
  starting transfers between devices  3.52 us (1%)
    all_gather x1, waiting for transfers between devices, sent_together(): result = lax.all_gather(both, axis, axis=dim, tiled=True)  68.8 us
    reduce_scatter x1, waiting for transfers between devices, shards(): lax.psum_scatter((jnp.dot(pool_out, out_pool_full, preferred_element_type...  57.4 us
    all_gather x1, waiting for transfers between devices, shards(): whole_rows = lax.all_gather(tokens, 'tp', axis=1, tiled=True)  26.8 us
    all_gather x2, waiting for transfers between devices, gather_axes(): nearer = lax.all_gather(array, axes[-1], axis=dim, tiled=True)  23.3 us
    all_gather x2, blocking collectives, gather_axes(): nearer = lax.all_gather(array, axes[-1], axis=dim, tiled=True)  23 us
    dot_general x4, matrix products, project(): return jnp.dot(normed, piece, preferred_element_type=jnp.float32)  13.9 us
    dot_general x1, matrix products, shards(): jnp.dot(attn_out, out_attn_full, preferred_element_type=jnp.float32)  12.1 us
    dot_general x1, matrix products, shards(): jnp.dot(pool_out, out_pool_full, preferred_element_type=jnp.float32)  10.7 us
  transfers between devices with their start and end apart: 7, of which 6 were waited for; matrix products, arithmetic and copies ran while one was open for 23% of the time, Pallas kernels for 0%

commit v1 on v0

--- a/solution.py
+++ b/solution.py
@@ -15,6 +15,23 @@
 epsilon = 1e-06
 rotary_base = 10000.0
 masked_score = -1e30
+
+
+def entries_play(vector, on_dim):
+    num_devices = lax.axis_size("tp")
+    pieces_in = tuple(((rr, (rr + 1) % num_devices) for rr in range(num_devices)))
+    by_rank = tuple(((rr, (rr - 1) % num_devices) for rr in range(num_devices)))
+    t_next, q_next = ([vector], [vector])
+    for _ in range(num_devices // 2):
+        val = lax.ppermute(t_next[-1], "tp", pieces_in)
+        t_next.append(val)
+    for _ in tuple(range((num_devices - 1) // 2)):
+        found_now = lax.ppermute(q_next[-1], "tp", by_rank)
+        q_next.append(found_now)
+    v_next = jnp.concatenate([*t_next[::-1], *q_next[1:]], axis=on_dim)
+    last = lax.axis_index("tp")
+    wide_out = jnp.roll(v_next, (last - num_devices // 2) * vector.shape[on_dim], axis=on_dim)
+    return wide_out
 
 
 def sent_together(arrays, axis, dim, along):
@@ -83,7 +100,7 @@
     out_pool_weight,
     out_attn_weight,
 ):
-    whole_rows = lax.all_gather(tokens, "tp", axis=1, tiled=True)
+    whole_rows = entries_play(tokens, 1)
     normed = rms_normed(whole_rows, norm_gain)
     tok_rows = normed.shape[0]
 

time: 307 us -> 261 us (0.85)
  waiting for transfers between devices: 178 us -> 93.3 us
  local copies, waits for them, and re-layouts: 8.52 us -> 32 us
  starting transfers between devices: 3.52 us -> 22.5 us
  other arithmetic: 28.3 us -> 18.3 us
  matrix products: 51.3 us -> 56.1 us
    all_gather x1, waiting for transfers between devices: 68.8 us -> 0.02 us  [sent_together(): result = lax.all_gather(both, axis, axis=dim, tiled=True)]
    ppermute x0 -> x7, waiting for transfers between devices: none -> 31.3 us  [the longest x4 22.9 us: entries_play(): val = lax.ppermute(t_next[-1], 'tp', pieces_in)]
    all_gather x1 -> x0, waiting for transfers between devices: 26.8 us -> none  [shards(): whole_rows = lax.all_gather(tokens, 'tp', axis=1, tiled=True)]
    unnamed x42 -> x61, local copies, waits for them, and re-layouts: 6.85 us -> 30.2 us
    all_gather x2, waiting for transfers between devices: 23.3 us -> 0.04 us  [gather_axes(): nearer = lax.all_gather(array, axes[-1], axis=dim, tiled=True)]
    ppermute x0 -> x7, starting transfers between devices: none -> 16.9 us  [the longest x4 8.61 us: entries_play(): val = lax.ppermute(t_next[-1], 'tp', pieces_in)]
    convert_element_type x1 -> x0, other arithmetic: 10.3 us -> none  [rms_normed(): return (scaled * gain).astype(jnp.bfloat16)]
    dot_general x4, matrix products: 13.9 us -> 18.9 us  [project(): return jnp.dot(normed, piece, preferred_element_type=jnp.float32)]
  transfers between devices with their start and end apart: 7 -> 13, of which waited for: 6 -> 5; matrix products, arithmetic and copies ran while one was open for 23% -> 29% of each run, Pallas kernels for 0% -> 0%
where the time goes in v1:
time: 261 us; the launch traced here: 260 us
  waiting for transfers between devices  93.3 us (36%)
  matrix products  56.1 us (21%)
  local copies, waits for them, and re-layouts  32 us (12%)
  blocking collectives  24 us (9%)
  starting transfers between devices  22.5 us (9%)
  other arithmetic  18.3 us (7%)
  between operations  13.8 us (5%)
    reduce_scatter x1, waiting for transfers between devices, shards(): lax.psum_scatter((jnp.dot(pool_out, out_pool_full, preferred_element_type...  61.8 us
    unnamed x61, local copies, waits for them, and re-layouts  30.2 us
    all_gather x2, blocking collectives, gather_axes(): nearer = lax.all_gather(array, axes[-1], axis=dim, tiled=True)  24 us
    ppermute x4, waiting for transfers between devices, entries_play(): val = lax.ppermute(t_next[-1], 'tp', pieces_in)  22.9 us
    dot_general x4, matrix products, project(): return jnp.dot(normed, piece, preferred_element_type=jnp.float32)  18.9 us
    dot_general x1, matrix products, shards(): jnp.dot(attn_out, out_attn_full, preferred_element_type=jnp.float32)  12.1 us
    dot_general x1, matrix products, shards(): jnp.dot(pool_out, out_pool_full, preferred_element_type=jnp.float32)  10.7 us
    dot_general x1, matrix products, shards(): jnp.einsum('kgqs,skd->qkgd', weights, value_pad, preferred_element_type=j...  9.31 us
  transfers between devices with their start and end apart: 13, of which 5 were waited for; matrix products, arithmetic and copies ran while one was open for 29% of the time, Pallas kernels for 0%

profile of v1, /device:TPU:1, one launch (start us, length us, event | category | flops | bytes accessed | tf_op | source)
XLA Modules:
  0.0 259.9 jit_solution(14632971366734640196)
XLA Ops:
  6.5 0.9 copy.17
  7.5 0.8 copy.18
  8.3 1.6 pad_maximum_fusion.2
  10.0 12.0 %all_gather.16 = bf16[256,512]{1,0:T(8,128)(2,1)} all-gather(bf16[256,128]{1,0:T(8,128)(2,1)} %param.20), channel_id=1, replica_groups=mesh['sp_0'=8,'sp_1'=4,'tp'=8] {'sp_1'}, dimensions={1}, use_global_device_ids=true | all-gather | bytes 327680 | tf_op jit(solution)/shard_map/all_gather | solution.py:60
  22.1 3.6 %collective-permute-start = (bf16[1024,512]{1,0:T(8,128)(2,1)}, bf16[1024,512]{1,0:T(8,128)(2,1)S(1)}, u32[]{:S(2)}, u32[]{:S(2)}) collective-permute-start(bf16[1024,512]{1,0:T(8,128)(2,1)} %param.11), channel_id=1, source_target_pairs={{0,1},{1,2},{2,3},{3,4},{4,5},{5,6},{6,7},{7,0},{8,9},{9,10},{10,1... | collective-permute-start | bytes 3145736 | tf_op jit(solution)/shard_map/ppermute | solution.py:26
  25.7 12.1 %collective-permute-done = bf16[1024,512]{1,0:T(8,128)(2,1)S(1)} collective-permute-done((bf16[1024,512]{1,0:T(8,128)(2,1)}, bf16[1024,512]{1,0:T(8,128)(2,1)S(1)}, u32[]{:S(2)}, u32[]{:S(2)}) %collective-permute-start) | collective-permute-done | bytes 1048608 | tf_op jit(solution)/shard_map/ppermute | solution.py:26
  37.8 2.4 collective-permute-start.1
  40.2 0.9 collective-permute-start.4
  41.1 10.8 %collective-permute-done.1 = bf16[1024,512]{1,0:T(8,128)(2,1)} collective-permute-done((bf16[1024,512]{1,0:T(8,128)(2,1)S(1)}, bf16[1024,512]{1,0:T(8,128)(2,1)}, u32[]{:S(2)}, u32[]{:S(2)}) %collective-permute-start.1) | collective-permute-done | bytes 1048608 | tf_op jit(solution)/shard_map/ppermute | solution.py:26
  51.9 2.6 collective-permute-start.2
  54.5 12.0 %all_gather.18 = bf16[256,512]{1,0:T(8,128)(2,1)} all-gather(bf16[256,128]{1,0:T(8,128)(2,1)} %param.21), channel_id=1, replica_groups=mesh['sp_0'=8,'sp_1'=4,'tp'=8] {'sp_1'}, dimensions={1}, use_global_device_ids=true | all-gather | bytes 327680 | tf_op jit(solution)/shard_map/all_gather | solution.py:60
  66.6 0.6 fusion.81
  67.2 0.6 subtract_convert_fusion.2
  67.8 0.7 broadcast_multiply_fusion.1
  68.5 4.6 %collective-permute-start.5 = (bf16[1024,512]{1,0:T(8,128)(2,1)S(1)}, bf16[1024,512]{1,0:T(8,128)(2,1)}, u32[]{:S(2)}, u32[]{:S(2)}) collective-permute-start(bf16[1024,512]{1,0:T(8,128)(2,1)S(1)} %collective-permute-done.4), channel_id=1, source_target_pairs={{0,7},{1,0},{2,1},{3,2},{4,3},{5,4},{6,5},{7,6},{8,15},{9,8},{10,9... | collective-permute-start | bytes 3145736 | tf_op jit(solution)/shard_map/ppermute | solution.py:29
  73.2 0.6 broadcast_compare_fusion
  73.8 0.6 subtract_convert_fusion.4
  74.4 1.1 fusion.76
  75.5 3.8 %fusion.7 = pred[1024,1280]{0,1:T(8,128)(4,1)} fusion(s32[1024]{0:T(1024)S(1)} %iota_add_fusion.1, s32[1280]{0:T(1024)S(1)} %iota_add_fusion, pred[1280]{0:T(1024)(128)(4,1)S(1)} %get-tuple-element.31, pred[1280]{0:T(1024)(128)(4,1)} %get-tuple-element.32), kind=kLoop, calls=%fused_computation.14 | loop fusion | flops 6553600 | bytes 1322496 | tf_op jit(solution)/shard_map/and | solution.py:166
  79.3 4.1 %collective-permute-done.5 = bf16[1024,512]{1,0:T(8,128)(2,1)} collective-permute-done((bf16[1024,512]{1,0:T(8,128)(2,1)S(1)}, bf16[1024,512]{1,0:T(8,128)(2,1)}, u32[]{:S(2)}, u32[]{:S(2)}) %collective-permute-start.5) | collective-permute-done | bytes 1048608 | tf_op jit(solution)/shard_map/ppermute | solution.py:29
  83.3 2.7 %collective-permute-start.6 = (bf16[1024,512]{1,0:T(8,128)(2,1)}, bf16[1024,512]{1,0:T(8,128)(2,1)S(1)}, u32[]{:S(2)}, u32[]{:S(2)}) collective-permute-start(bf16[1024,512]{1,0:T(8,128)(2,1)} %collective-permute-done.5), channel_id=1, source_target_pairs={{0,7},{1,0},{2,1},{3,2},{4,3},{5,4},{6,5},{7,6},{8,15},{9,8},{10,9... | collective-permute-start | bytes 3145736 | tf_op jit(solution)/shard_map/ppermute | solution.py:29
  86.1 0.6 broadcast_compare_fusion.2
  86.7 1.4 constant_dynamic-update-slice_fusion.15
  88.0 1.4 constant_dynamic-update-slice_fusion.14
  89.4 1.4 constant_dynamic-update-slice_fusion.13
  90.8 0.1 constant_dynamic-update-slice_fusion.12
  90.9 1.4 constant_dynamic-update-slice_fusion.11
  92.3 0.1 constant_dynamic-update-slice_fusion.10
  92.4 1.4 constant_dynamic-update-slice_fusion.9
  93.8 4.4 %collective-permute-done.6 = bf16[1024,512]{1,0:T(8,128)(2,1)S(1)} collective-permute-done((bf16[1024,512]{1,0:T(8,128)(2,1)}, bf16[1024,512]{1,0:T(8,128)(2,1)S(1)}, u32[]{:S(2)}, u32[]{:S(2)}) %collective-permute-start.6) | collective-permute-done | bytes 1048608 | tf_op jit(solution)/shard_map/ppermute | solution.py:29
  98.2 0.1 constant_dynamic-update-slice_fusion.8
  98.3 1.4 constant_dynamic-update-slice_fusion.7
  99.7 1.3 constant_dynamic-update-slice_fusion.6
  101.0 1.3 constant_dynamic-update-slice_fusion.5
  102.4 0.1 constant_dynamic-update-slice_fusion.4
  102.7 0.1 constant_dynamic-update-slice_fusion.2
  102.8 1.3 constant_dynamic-update-slice_fusion.1
  104.2 0.1 constant_dynamic-update-slice_fusion
  104.3 5.8 %copy-done.2 = bf16[1024,8192]{1,0:T(8,128)(2,1)} copy-done((bf16[1024,8192]{1,0:T(8,128)(2,1)}, bf16[1024,8192]{1,0:T(8,128)(2,1)S(1)}, u32[]{:S(2)}) %copy-start.2) | copy-done | bytes 16777240
  110.1 1.7 fusion.1
  111.9 5.9 %fusion.33 = f32[1024,64]{0,1:T(8,128)S(1)} fusion(bf16[4096,640]{1,0:T(8,128)(2,1)} %all-gather.4.cloned.1.call-done, f32[4096]{0:T(1024)S(1)} %copy-done.21, f32[1024]{0:T(1024)S(1)} %add_rsqrt_fusion, bf16[1024,8192]{1,0:T(8,128)(2,1)} %copy-done.2, s32[]{:T(128)S(6)} %select_n.89), kind=kOutput, calls=%fused_computation.42 | convolution fusion | flops 553648128 | bytes 9719812 | tf_op jit(solution)/shard_map/dot_general | solution.py:108
  117.8 0.5 subtract_convert_fusion.1
  118.3 2.3 copy-done.3
  120.6 4.1 %convolution_convert_fusion = bf16[1024,64]{0,1:T(8,128)(2,1)S(1)} fusion(bf16[4096,640]{1,0:T(8,128)(2,1)} %all-gather.4.cloned.1.call-done, f32[4096]{0:T(1024)S(1)} %copy-done.21, f32[1024]{0:T(1024)S(1)} %add_rsqrt_fusion, bf16[1024,8192]{1,0:T(8,128)(2,1)S(1)} %copy-done.3, s32[]{:T(128)S(6)} %select_n.89), kind=kOutput, calls=%fused_computation.27 | convolution fusion | flops 553713664 | bytes 9588740 | tf_op jit(solution)/shard_map/dot_general | solution.py:108
  124.7 4.5 %fusion.14 = bf16[1024,256]{0,1:T(8,128)(2,1)S(1)} fusion(bf16[4096,640]{1,0:T(8,128)(2,1)} %all-gather.4.cloned.1.call-done, f32[4096]{0:T(1024)S(1)} %copy-done.21, f32[1024]{0:T(1024)S(1)} %add_rsqrt_fusion, bf16[1024,8192]{1,0:T(8,128)(2,1)S(1)} %copy-done.3, s32[]{:T(128)S(6)} %select_n.89), kind=kOutput, calls=%fused_computation.22 | convolution fusion | flops 2164523008 | bytes 11030532 | tf_op jit(solution)/shard_map/dot_general | solution.py:108
  129.3 4.0 %collective-permute-start.7 = (bf16[128,384]{0,1:T(8,128)(2,1)S(1)}, bf16[128,384]{0,1:T(8,128)(2,1)S(1)}, u32[]{:S(2)}, u32[]{:S(2)}) collective-permute-start(bf16[128,384]{0,1:T(8,128)(2,1)S(1)} %get-tuple-element.7), channel_id=1, source_target_pairs={{0,8},{8,16},{16,24},{24,32},{32,40},{40,48},{48,56},{56,64},{64,7... | collective-permute-start | bytes 294920 | tf_op jit(solution)/shard_map/ppermute | solution.py:49
  133.2 1.5 collective-permute-start.8
  134.7 4.4 %fusion.8 = f32[1024,256]{0,1:T(8,128)S(1)} fusion(bf16[4096,640]{1,0:T(8,128)(2,1)} %all-gather.4.cloned.1.call-done, f32[4096]{0:T(1024)S(1)} %copy-done.21, f32[1024]{0:T(1024)S(1)} %add_rsqrt_fusion, bf16[1024,8192]{1,0:T(8,128)(2,1)S(1)} %copy-done.3, s32[]{:T(128)S(6)} %select_n.89), kind=kOutput, calls=%fused_computation.15 | convolution fusion | flops 2164260864 | bytes 11554820 | tf_op jit(solution)/shard_map/dot_general | solution.py:108
  139.1 0.2 subtract_convert_fusion
  139.3 0.9 pad_maximum_fusion.1
  140.3 0.2 slice_bitcast_fusion
  140.6 0.2 copy-done.12
  140.9 0.4 copy.19
  141.3 1.3 fusion.12
  142.6 0.2 broadcast_add_fusion
  142.8 5.1 %fusion.100 = (f32[4,1024]{1,0:T(4,128)S(1)}, f32[1,4,1024,1280]{2,3,1,0:T(8,128)S(1)}) fusion(bf16[1024,4,64]{0,2,1:T(8,128)(2,1)} %bitcast.57, bf16[128,384]{0,1:T(8,128)(2,1)} %copy-done.14, bf16[128,384]{0,1:T(8,128)(2,1)} %copy-done.12, bf16[1024,64]{0,1:T(8,128)(2,1)} %copy-done.8, bf16[1024,64]{0,1:T(8,128)(2,1)S(1)} %bitcast.54, ...), kind=kOutput, calls=%fused_computation.156 | convolution fusion | flops 687632384 | bytes 23805952 | tf_op jit(solution)/shard_map/qkgd,skd->kgqs/dot_general | solution.py:161
  148.1 7.1 %copy-done.1 = f32[1,4,1024,1280]{2,3,1,0:T(8,128)} copy-done((f32[1,4,1024,1280]{2,3,1,0:T(8,128)}, f32[1,4,1024,1280]{2,3,1,0:T(8,128)S(1)}, u32[]{:S(2)}) %copy-start.1) | copy-done | bytes 20971544
  155.2 2.9 %fusion = f32[4,1024]{1,0:T(4,128)S(1)} fusion(f32[1,4,1024,1280]{2,3,1,0:T(8,128)S(1)} %get-tuple-element.20, f32[4,1024]{1,0:T(4,128)S(1)} %broadcast_maximum_fusion), kind=kLoop, calls=%fused_computation.5 | loop fusion | flops 10481664 | bytes 21004288 | tf_op jit(solution)/shard_map/reduce_sum | solution.py:174
  158.3 0.7 copy.21
  159.0 0.4 copy.22
  159.4 10.7 %fusion.21 = f32[1024,4096]{1,0:T(8,128)} fusion(bf16[256,4096]{1,0:T(8,128)(2,1)} %all-gather.6.cloned.1.call-done, bf16[1024,256]{0,1:T(8,128)(2,1)S(1)} %copy-done.6, f32[1152,256]{0,1:T(8,128)S(1)} %bitcast.50, f32[1040,256]{0,1:T(8,128)S(1)} %bitcast.51, f32[256]{0:T(256)} %param.18, f32[1024]{0:T(1024)S(1)} %copy-done.16, f32[1024]{0:T(1024)S(1)} %copy-done.17, ...), kind=kOutput, calls=%fused_computation.25 | convolution fusion | flops 2286157824 | bytes 28067840 | tf_op jit(solution)/shard_map/dot_general | solution.py:184
  170.1 9.3 %fusion.18 = bf16[64,4,1024]{2,0,1:T(8,128)(2,1)S(1)} fusion(f32[4,1024]{1,0:T(4,128)S(1)} %exponential_add_fusion, f32[1,4,1024,1280]{2,3,1,0:T(8,128)} %copy-done.1, f32[4,1024]{1,0:T(4,128)S(1)} %broadcast_maximum_fusion, bf16[128,384]{0,1:T(8,128)(2,1)S(1)} %copy-done.15, bf16[128,384]{0,1:T(8,128)(2,1)S(1)} %copy-done.13, ...), kind=kOutput, calls=%fused_computation.24 | convolution fusion | flops 687898624 | bytes 22511616 | tf_op jit(solution)/shard_map/kgqs,skd->qkgd/dot_general | solution.py:176
  179.4 12.1 %add_convert_fusion = bf16[1024,4096]{1,0:T(8,128)(2,1)} fusion(f32[1024,4096]{1,0:T(8,128)} %fusion.21, bf16[1024,256]{0,1:T(8,128)(2,1)S(1)} %bitcast.49, bf16[256,4096]{1,0:T(8,128)(2,1)} %all-gather.8.cloned.1.call-done), kind=kOutput, calls=%fused_computation.9 | convolution fusion | flops 2155872256 | bytes 27787264 | tf_op jit(solution)/shard_map/dot_general | solution.py:185
  191.6 61.8 %reduce-scatter.2.cloned.1.call-done = bf16[128,4096]{1,0:T(8,128)(2,1)} async-done(((bf16[1024,4096]{1,0:T(8,128)(2,1)}), bf16[128,4096]{1,0:T(8,128)(2,1)}) %reduce-scatter.2.cloned.1.call-update) | async-done | bytes 1048592 | tf_op jit(solution)/shard_map/reduce_scatter | solution.py:182
  (71 shorter events, 1.0 us)
Async XLA Ops:
  6.5 152.8 %copy-start = (bf16[1,256,256]{2,1,0:T(8,128)(2,1)S(1)}, bf16[1,256,256]{2,1,0:T(8,128)(2,1)}, u32[]{:S(2)}) copy-start(bf16[1,256,256]{2,1,0:T(8,128)(2,1)} %param.17) | copy-start | bytes 393220
  6.5 96.0 %copy-start.4 = (bf16[1024,512]{1,0:T(8,128)(2,1)S(1)}, bf16[1024,512]{1,0:T(8,128)(2,1)}, u32[]{:S(2)}) copy-start(bf16[1024,512]{1,0:T(8,128)(2,1)} %param.11) | copy-start | bytes 3145732
  6.5 105.3 %all-gather.4.cloned.1.call-start = ((), (), s32[]{:S(2)}) async-start(), calls=%async_computation.1 | async-start | bytes 5406720 | tf_op jit(solution)/shard_map/all_gather | solution.py:40
  10.0 149.4 %all-gather.6.cloned.1.call-start = ((), (), s32[]{:S(2)}) async-start(), calls=%async_computation.2 | async-start | bytes 2359296 | tf_op jit(solution)/shard_map/all_gather | solution.py:60
  22.0 157.4 %all-gather.8.cloned.1.call-start = ((), (), s32[]{:S(2)}) async-start(), calls=%async_computation.3 | async-start | bytes 2359296 | tf_op jit(solution)/shard_map/all_gather | solution.py:60
  22.1 15.7 %collective-permute-start = (bf16[1024,512]{1,0:T(8,128)(2,1)}, bf16[1024,512]{1,0:T(8,128)(2,1)S(1)}, u32[]{:S(2)}, u32[]{:S(2)}) collective-permute-start(bf16[1024,512]{1,0:T(8,128)(2,1)} %param.11), channel_id=1, source_target_pairs={{0,1},{1,2},{2,3},{3,4},{4,5},{5,6},{6,7},{7,0},{8,9},{9,10},{10,1... | collective-permute-start | bytes 3145736 | tf_op jit(solution)/shard_map/ppermute | solution.py:26
  37.8 14.1 %collective-permute-start.1 = (bf16[1024,512]{1,0:T(8,128)(2,1)S(1)}, bf16[1024,512]{1,0:T(8,128)(2,1)}, u32[]{:S(2)}, u32[]{:S(2)}) collective-permute-start(bf16[1024,512]{1,0:T(8,128)(2,1)S(1)} %collective-permute-done), channel_id=1, source_target_pairs={{0,1},{1,2},{2,3},{3,4},{4,5},{5,6},{6,7},{7,0},{8,9},{9,10},{10,1... | collective-permute-start | bytes 3145736 | tf_op jit(solution)/shard_map/ppermute | solution.py:26
  40.2 28.4 %collective-permute-start.4 = (bf16[1024,512]{1,0:T(8,128)(2,1)}, bf16[1024,512]{1,0:T(8,128)(2,1)S(1)}, u32[]{:S(2)}, u32[]{:S(2)}) collective-permute-start(bf16[1024,512]{1,0:T(8,128)(2,1)} %param.11), channel_id=1, source_target_pairs={{0,7},{1,0},{2,1},{3,2},{4,3},{5,4},{6,5},{7,6},{8,15},{9,8},{10,9... | collective-permute-start | bytes 3145736 | tf_op jit(solution)/shard_map/ppermute | solution.py:29
  51.9 21.3 %collective-permute-start.2 = (bf16[1024,512]{1,0:T(8,128)(2,1)}, bf16[1024,512]{1,0:T(8,128)(2,1)}, u32[]{:S(2)}, u32[]{:S(2)}) collective-permute-start(bf16[1024,512]{1,0:T(8,128)(2,1)} %collective-permute-done.1), channel_id=1, source_target_pairs={{0,1},{1,2},{2,3},{3,4},{4,5},{5,6},{6,7},{7,0},{8,9},{9,10},{10,1... | collective-permute-start | bytes 3145736 | tf_op jit(solution)/shard_map/ppermute | solution.py:26
  66.5 186.9 %reduce-scatter.2.cloned.1.call-start = ((), (), s32[]{:S(2)}) async-start(), calls=%async_computation.4 | async-start | bytes 9437184 | tf_op jit(solution)/shard_map/reduce_scatter | solution.py:182
  68.5 14.8 %collective-permute-start.5 = (bf16[1024,512]{1,0:T(8,128)(2,1)S(1)}, bf16[1024,512]{1,0:T(8,128)(2,1)}, u32[]{:S(2)}, u32[]{:S(2)}) collective-permute-start(bf16[1024,512]{1,0:T(8,128)(2,1)S(1)} %collective-permute-done.4), channel_id=1, source_target_pairs={{0,7},{1,0},{2,1},{3,2},{4,3},{5,4},{6,5},{7,6},{8,15},{9,8},{10,9... | collective-permute-start | bytes 3145736 | tf_op jit(solution)/shard_map/ppermute | solution.py:29
  73.2 13.5 %collective-permute-start.3 = (bf16[1024,512]{1,0:T(8,128)(2,1)}, bf16[1024,512]{1,0:T(8,128)(2,1)}, u32[]{:S(2)}, u32[]{:S(2)}) collective-permute-start(bf16[1024,512]{1,0:T(8,128)(2,1)} %collective-permute-done.2), channel_id=1, source_target_pairs={{0,1},{1,2},{2,3},{3,4},{4,5},{5,6},{6,7},{7,0},{8,9},{9,10},{10,1... | collective-permute-start | bytes 3145736 | tf_op jit(solution)/shard_map/ppermute | solution.py:26
  83.3 14.8 %collective-permute-start.6 = (bf16[1024,512]{1,0:T(8,128)(2,1)}, bf16[1024,512]{1,0:T(8,128)(2,1)S(1)}, u32[]{:S(2)}, u32[]{:S(2)}) collective-permute-start(bf16[1024,512]{1,0:T(8,128)(2,1)} %collective-permute-done.5), channel_id=1, source_target_pairs={{0,7},{1,0},{2,1},{3,2},{4,3},{5,4},{6,5},{7,6},{8,15},{9,8},{10,9... | collective-permute-start | bytes 3145736 | tf_op jit(solution)/shard_map/ppermute | solution.py:29
  90.9 20.9 %copy-start.21 = (f32[4096]{0:T(1024)S(1)}, f32[4096]{0:T(1024)}, u32[]{:S(2)}) copy-start(f32[4096]{0:T(1024)} %param.12) | copy-start | bytes 49156
  104.2 13.6 %copy-start.10 = (f32[1024,1,1,1,16]{0,4,3,2,1:T(8,128)S(1)}, f32[1024,1,1,1,16]{0,4,3,2,1:T(8,128)}, u32[]{:S(2)}) copy-start(f32[1024,1,1,1,16]{0,4,3,2,1:T(8,128)} %get-tuple-element.14) | copy-start | bytes 196612
  104.2 13.6 %copy-start.11 = (f32[1024,1,1,1,16]{0,4,3,2,1:T(8,128)S(1)}, f32[1024,1,1,1,16]{0,4,3,2,1:T(8,128)}, u32[]{:S(2)}) copy-start(f32[1024,1,1,1,16]{0,4,3,2,1:T(8,128)} %get-tuple-element.17) | copy-start | bytes 196612
  104.3 5.8 %copy-start.2 = (bf16[1024,8192]{1,0:T(8,128)(2,1)}, bf16[1024,8192]{1,0:T(8,128)(2,1)S(1)}, u32[]{:S(2)}) copy-start(bf16[1024,8192]{1,0:T(8,128)(2,1)S(1)} %constant_dynamic-update-slice_fusion) | copy-start | bytes 50331652
  111.8 8.7 %copy-start.3 = (bf16[1024,8192]{1,0:T(8,128)(2,1)S(1)}, bf16[1024,8192]{1,0:T(8,128)(2,1)}, u32[]{:S(2)}) copy-start(bf16[1024,8192]{1,0:T(8,128)(2,1)} %copy-done.2) | copy-start | bytes 50331652
  124.7 15.5 %copy-start.8 = (bf16[1024,64]{0,1:T(8,128)(2,1)}, bf16[1024,64]{0,1:T(8,128)(2,1)S(1)}, u32[]{:S(2)}) copy-start(bf16[1024,64]{0,1:T(8,128)(2,1)S(1)} %convolution_convert_fusion) | copy-start | bytes 393220
  129.2 11.4 %copy-start.5 = (bf16[1024,256]{0,1:T(8,128)(2,1)}, bf16[1024,256]{0,1:T(8,128)(2,1)S(1)}, u32[]{:S(2)}) copy-start(bf16[1024,256]{0,1:T(8,128)(2,1)S(1)} %fusion.14) | copy-start | bytes 1572868
  129.2 9.9 %copy-start.7 = (f32[1024,2,16]{0,2,1:T(8,128)S(1)}, f32[1024,2,16]{0,2,1:T(8,128)}, u32[]{:S(2)}) copy-start(f32[1024,2,16]{0,2,1:T(8,128)} %get-tuple-element.12) | copy-start | bytes 393220
  129.3 10.9 %collective-permute-start.7 = (bf16[128,384]{0,1:T(8,128)(2,1)S(1)}, bf16[128,384]{0,1:T(8,128)(2,1)S(1)}, u32[]{:S(2)}, u32[]{:S(2)}) collective-permute-start(bf16[128,384]{0,1:T(8,128)(2,1)S(1)} %get-tuple-element.7), channel_id=1, source_target_pairs={{0,8},{8,16},{16,24},{24,32},{32,40},{40,48},{48,56},{56,64},{64,7... | collective-permute-start | bytes 294920 | tf_op jit(solution)/shard_map/ppermute | solution.py:49
  133.2 6.9 %collective-permute-start.8 = (bf16[128,384]{0,1:T(8,128)(2,1)S(1)}, bf16[128,384]{0,1:T(8,128)(2,1)S(1)}, u32[]{:S(2)}, u32[]{:S(2)}) collective-permute-start(bf16[128,384]{0,1:T(8,128)(2,1)S(1)} %get-tuple-element.8), channel_id=1, source_target_pairs={{8,0},{16,8},{24,16},{32,24},{40,32},{48,40},{56,48},{64,56},{72,6... | collective-permute-start | bytes 294920 | tf_op jit(solution)/shard_map/ppermute | solution.py:52
  140.2 0.6 copy-start.12
  140.2 0.6 copy-start.14
  142.8 5.2 %copy-start.20 = (f32[4]{0:T(128)S(1)}, f32[4]{0:T(128)}, u32[]{:S(2)}) copy-start(f32[4]{0:T(128)} %param.19) | copy-start | bytes 52
  148.0 7.2 %copy-start.1 = (f32[1,4,1024,1280]{2,3,1,0:T(8,128)}, f32[1,4,1024,1280]{2,3,1,0:T(8,128)S(1)}, u32[]{:S(2)}) copy-start(f32[1,4,1024,1280]{2,3,1,0:T(8,128)S(1)} %get-tuple-element.20) | copy-start | bytes 62914564
  148.0 11.4 %copy-start.6 = (bf16[1024,256]{0,1:T(8,128)(2,1)S(1)}, bf16[1024,256]{0,1:T(8,128)(2,1)}, u32[]{:S(2)}) copy-start(bf16[1024,256]{0,1:T(8,128)(2,1)} %copy-done.5) | copy-start | bytes 1572868
  148.0 11.4 %copy-start.16 = (f32[1024]{0:T(1024)S(1)}, f32[1024]{0:T(1024)}, u32[]{:S(2)}) copy-start(f32[1024]{0:T(1024)} %get-tuple-element.27) | copy-start | bytes 12292
  148.0 11.4 %copy-start.17 = (f32[1024]{0:T(1024)S(1)}, f32[1024]{0:T(1024)}, u32[]{:S(2)}) copy-start(f32[1024]{0:T(1024)} %get-tuple-element.28) | copy-start | bytes 12292
  148.0 11.4 %copy-start.18 = (f32[1024]{0:T(1024)S(1)}, f32[1024]{0:T(1024)}, u32[]{:S(2)}) copy-start(f32[1024]{0:T(1024)} %get-tuple-element.29) | copy-start | bytes 12292
  148.1 11.4 %copy-start.19 = (f32[1024]{0:T(1024)S(1)}, f32[1024]{0:T(1024)}, u32[]{:S(2)}) copy-start(f32[1024]{0:T(1024)} %get-tuple-element.30) | copy-start | bytes 12292
  158.2 11.9 %copy-start.9 = (bf16[1024,64]{0,1:T(8,128)(2,1)S(1)}, bf16[1024,64]{0,1:T(8,128)(2,1)}, u32[]{:S(2)}) copy-start(bf16[1024,64]{0,1:T(8,128)(2,1)} %copy-done.8) | copy-start | bytes 393220
  158.2 11.9 %copy-start.13 = (bf16[128,384]{0,1:T(8,128)(2,1)S(1)}, bf16[128,384]{0,1:T(8,128)(2,1)}, u32[]{:S(2)}) copy-start(bf16[128,384]{0,1:T(8,128)(2,1)} %copy-done.12) | copy-start | bytes 294916
  158.2 11.9 %copy-start.15 = (bf16[128,384]{0,1:T(8,128)(2,1)S(1)}, bf16[128,384]{0,1:T(8,128)(2,1)}, u32[]{:S(2)}) copy-start(bf16[128,384]{0,1:T(8,128)(2,1)} %copy-done.14) | copy-start | bytes 294916
Sparse Core Ops, SparseCore 0:
  10.1 87.7 all-gather.3
  99.7 35.3 all-gather.5
  136.9 39.3 all-gather.7
  191.7 61.6 reduce-scatter.1
